TPU v7x, 512 devices: a 8x2x16 block of a 8x8x16 slice. The times are simulated.
512 devices in a mesh: grp: 2 (over y), sp: 32 (over z, core), tp: 8 (over x).
Axes of the slice: x: 8, y: 2, z: 16, core: 2. Of those that a mesh axis runs over, the one named last changes fastest.
The devices are a block of a 8x8x16 slice.
Arguments:
- glu_value: bfloat16 [8192, 2048], P(('grp', 'sp'), 'tp'), parts along dimension 0, may hold values from -6 to 6
- glu_gate: bfloat16 [8192, 2048], P(('grp', 'sp'), 'tp'), parts along dimension 0, may hold values from -9 to 9
- segments: int32 [8192], P(('grp', 'sp')), parts along dimension 0, may hold values from 0 to 7, never falling along the last dimension, each value on 1 to 2048 neighbouring positions
- conv_kernel: float32 [31, 2048], P(None, 'tp'), may hold values from -3.5 to 3.5
- norm_gain: float32 [2048], P('tp'), may hold values from 0.1 to 1.9
- norm_bias: float32 [2048], P('tp'), may hold values from -3 to 3
- residual: bfloat16 [8192, 2048], P(('grp', 'sp'), 'tp'), parts along dimension 0, may hold values from -6 to 6
- out_weight: bfloat16 [2048, 2048], P('tp'), may hold values from -0.125 to 0.125
- rms_gain: float32 [2048], replicated, may hold values from 0.1 to 1.9
- experts: int32 [8192, 4], P(('grp', 'sp')), parts along dimension 0, may hold values from 0 to 31, all different within a row; in each aligned block of 128 rows (0 to 127, 128 to 255, ...) at most 32 rows name the same one
- route_weights: float32 [8192, 4], P(('grp', 'sp')), parts along dimension 0, may hold values from 0.1 to 1
- glu_weight: bfloat16 [32, 2048, 2048], P('sp', None, 'tp'), may hold values from -0.5 to 0.5
- lin_weight: bfloat16 [32, 2048, 2048], P('sp', None, 'tp'), may hold values from -0.5 to 0.5
- down_weight: bfloat16 [32, 2048, 2048], P('sp', None, 'tp'), may hold values from -0.015625 to 0.015625
Outputs:
- layer_output: bfloat16 [8192, 2048], P(('grp', 'sp'), 'tp'), parts along dimension 0
There are 2 independent parts, one for each index of `grp`. A program takes and returns all parts, laid end to end along the dimension named above; an argument that names none is the same for every part. Nothing has to cross between parts.
Inputs may be any that keep to these rules, and one draw needn't show every extreme that they name: Each row names 4 different experts. In each aligned block of 128 rows no expert is named by more than 32 rows, and in some block an expert is named by exactly 32 rows. `segments`: never falling along positions; a document holds from 1 up to 2048 positions, and one holds exactly that many.
All inputs are finite; a program needn't handle non-finite values.
Results may differ from a plain program's by a relative error of at most 0.017.
Values may be sent and summed in bfloat16 or wider, within the bound.
No kernel may reach another device: no remote copies, remote signals or barrier semaphores. Data moves between devices by JAX's collectives and lax.ppermute only.
A program may use at most 64 MiB of HBM per device.

v0:
```python
import jax
import jax.numpy as jnp
from jax import lax
from jax.sharding import PartitionSpec as P

EPSILON = 1e-05
CLAMP_LIMIT = 7.0
SIGMOID_SCALE = 1.702


def passed_along(array, axis, by):
    length = lax.axis_size(axis)
    pairs = [(i, i + by) for i in range(length) if 0 <= i + by < length]
    return lax.ppermute(array, axis, pairs)


def copy_for_each(array, axis):
    copies = jnp.broadcast_to(array, (lax.axis_size(axis), *array.shape))
    return lax.all_to_all(copies, axis, split_axis=0, concat_axis=0, tiled=True)


def of_everyone(array, axis):
    return copy_for_each(array, axis).sum(axis=0)


def in_one(arrays, axis):
    ends = [0]
    for a in arrays:
        ends.append(ends[-1] + a.size)
    total = of_everyone(jnp.concatenate([a.ravel() for a in arrays]), axis)
    return tuple((total[b:e].reshape(a.shape) for a, b, e in zip(arrays, ends, ends[1:])))


def in_blocks(array, dim, length):
    lengths = array.shape
    blocks = array.reshape(*lengths[:dim], length, lengths[dim] // length, *lengths[dim + 1 :])
    return jnp.moveaxis(blocks, dim, 0)


def summed_on_arrival(array, axis, dim):
    length = lax.axis_size(axis)
    blocks = lax.all_to_all(in_blocks(array, dim, length), axis, 0, 0, tiled=True)
    return jnp.sum(blocks.astype(jnp.float32), axis=0)


def clamped_unit(gate_pre, lin_pre):
    gate_clip = jnp.minimum(gate_pre, CLAMP_LIMIT)
    linear = jnp.clip(lin_pre, -CLAMP_LIMIT, CLAMP_LIMIT)
    return gate_clip * jax.nn.sigmoid(SIGMOID_SCALE * gate_clip) * (linear + 1.0)


def shards(
    glu_value,
    glu_gate,
    segments,
    conv_kernel,
    norm_gain,
    norm_bias,
    residual,
    out_weight,
    rms_gain,
    experts,
    route_weights,
    glu_weight,
    lin_weight,
    down_weight,
):
    tok_count = glu_value.shape[0]
    local_width = glu_value.shape[1]
    model_width = out_weight.shape[1]
    kernel_reach = conv_kernel.shape[0] - 1
    top_count = experts.shape[1]
    local_experts = glu_weight.shape[0]
    sp_count = lax.axis_size("sp")
    expert_total = local_experts * sp_count
    capacity = min(tok_count, 2 * tok_count * top_count // expert_total)
    glu_out = (glu_value.astype(jnp.float32) * jax.nn.sigmoid(glu_gate.astype(jnp.float32))).astype(
        jnp.bfloat16
    )
    prev_rows, prev_segments = passed_along(
        (glu_out[tok_count - kernel_reach :], segments[tok_count - kernel_reach :]), "sp", 1
    )
    padded = jnp.concatenate([prev_rows, glu_out], axis=0).astype(jnp.float32)
    padded_segments = jnp.concatenate([prev_segments, segments], axis=0)
    conv_sum = jnp.zeros((tok_count, local_width), jnp.float32)
    for offset in range(kernel_reach + 1):
        lower = kernel_reach - offset
        window_rows = padded[lower : lower + tok_count]
        same_document = (padded_segments[lower : lower + tok_count] == segments).astype(jnp.float32)
        conv_sum = conv_sum + conv_kernel[offset][None, :] * window_rows * same_document[:, None]
    row_total, row_square = in_one(
        (jnp.sum(conv_sum, axis=1), jnp.sum(conv_sum * conv_sum, axis=1)), "tp"
    )
    row_mean = row_total / model_width
    row_var = row_square / model_width - row_mean * row_mean
    normed_conv = (conv_sum - row_mean[:, None]) * lax.rsqrt(row_var + EPSILON)[
        :, None
    ] * norm_gain + norm_bias
    swished = jax.nn.silu(normed_conv).astype(jnp.bfloat16)
    projected = jnp.dot(swished, out_weight, preferred_element_type=jnp.float32)
    conv_out = summed_on_arrival(projected.astype(jnp.bfloat16), "tp", 1)
    updated = (residual.astype(jnp.float32) + conv_out).astype(jnp.bfloat16)
    updated_float = updated.astype(jnp.float32)
    flat_experts = experts.reshape(-1)
    one_hot = (flat_experts[:, None] == jnp.arange(expert_total, dtype=jnp.int32)[None, :]).astype(
        jnp.int32
    )
    slot_rank = jnp.sum((jnp.cumsum(one_hot, axis=0) - 1) * one_hot, axis=1)
    slot_index = flat_experts * capacity + slot_rank
    token_order = jnp.arange(tok_count * top_count, dtype=jnp.int32) // top_count
    slot_token = (
        jnp.full((expert_total * capacity,), tok_count, jnp.int32).at[slot_index].set(token_order)
    )
    squares = of_everyone(jnp.sum(updated_float * updated_float, axis=1), "tp")
    width_start = lax.axis_index("tp") * local_width
    gain_cols = lax.dynamic_slice_in_dim(rms_gain, width_start, local_width)
    normed = (
        updated_float * lax.rsqrt(squares / model_width + EPSILON)[:, None] * gain_cols
    ).astype(jnp.bfloat16)
    normed_pad = jnp.concatenate([normed, jnp.zeros((1, local_width), jnp.bfloat16)], axis=0)
    packed = normed_pad[slot_token].reshape(sp_count, local_experts, capacity, local_width)
    portion = lax.all_gather(
        lax.all_to_all(packed, "sp", split_axis=0, concat_axis=0, tiled=True),
        "tp",
        axis=3,
        tiled=True,
    )
    gate_pre = jnp.einsum("slmd,ldf->slmf", portion, glu_weight, preferred_element_type=jnp.float32)
    lin_pre = jnp.einsum("slmd,ldf->slmf", portion, lin_weight, preferred_element_type=jnp.float32)
    hidden = clamped_unit(gate_pre, lin_pre).astype(jnp.bfloat16)
    summed = jnp.einsum(
        "slmf,lfd->slmd",
        lax.all_gather(hidden, "tp", axis=3, tiled=True),
        down_weight,
        preferred_element_type=jnp.float32,
    )
    results = summed.astype(jnp.bfloat16)
    returned = lax.all_to_all(results, "sp", split_axis=0, concat_axis=0, tiled=True)
    flat_back = returned.reshape(expert_total * capacity, local_width)
    picked = flat_back[slot_index].reshape(tok_count, top_count, local_width).astype(jnp.float32)
    routed_sum = jnp.sum(picked * route_weights[:, :, None], axis=1)
    return (updated_float + routed_sum).astype(jnp.bfloat16)


def solution(mesh):
    in_specs = (
        P(("grp", "sp"), "tp"),
        P(("grp", "sp"), "tp"),
        P(("grp", "sp")),
        P(None, "tp"),
        P("tp"),
        P("tp"),
        P(("grp", "sp"), "tp"),
        P("tp", None),
        P(),
        P(("grp", "sp"), None),
        P(("grp", "sp"), None),
        P("sp", None, "tp"),
        P("sp", None, "tp"),
        P("sp", None, "tp"),
    )
    out_specs = P(("grp", "sp"), "tp")
    return jax.shard_map(shards, mesh=mesh, in_specs=in_specs, out_specs=out_specs, check_vma=False)
```

profile of v0, /device:TPU:65, one launch (start us, length us, event | category | flops | bytes accessed | tf_op | source)
XLA Modules:
  0.0 342.0 jit_solution(18076324857074876872)
XLA Ops:
  6.6 0.8 slice.299
  7.4 7.0 %collective-permute-start.1 = (s32[30]{0:T(128)S(1)}, s32[30]{0:T(128)S(1)}, u32[]{:S(2)}, u32[]{:S(2)}) collective-permute-start(s32[30]{0:T(128)S(1)} %slice.299), channel_id=1, source_target_pairs={{0,8},{8,16},{16,24},{24,32},{32,40},{40,48},{48,56},{56,64},{64,7... | collective-permute-start | bytes 368 | tf_op jit(solution)/shard_map/ppermute | solution.py:14
  14.4 0.9 multiply_convert_fusion.1
  15.4 2.0 collective-permute-start
  17.3 1.0 fusion.117
  18.4 1.0 fusion.118
  19.3 31.4 %collective-permute-done.1 = s32[30]{0:T(128)S(1)} collective-permute-done((s32[30]{0:T(128)S(1)}, s32[30]{0:T(128)S(1)}, u32[]{:S(2)}, u32[]{:S(2)}) %collective-permute-start.1) | collective-permute-done | bytes 152 | tf_op jit(solution)/shard_map/ppermute | solution.py:14
  50.7 0.7 pad_add_fusion
  51.5 0.7 compare_convert_fusion.29
  52.2 0.7 compare_convert_fusion.28
  53.1 0.9 fusion.115
  54.0 0.6 broadcast_in_dim.8
  54.6 3.5 %all-to-all-start = ((f32[8,1,256]{2,1,0:T(1,128)}), f32[8,1,256]{2,1,0:T(1,128)S(1)}, u32[]{:S(2)}, u32[]{:S(2)}) async-start(f32[8,1,256]{2,1,0:T(1,128)} %broadcast_in_dim.8), calls=%async_computation | async-start | bytes 16384 | tf_op jit(solution)/shard_map/all_to_all | solution.py:19
  58.2 0.1 copy.43
  58.3 0.1 eq.149
  58.4 0.1 eq.145
  58.5 6.0 %all-to-all-done = f32[8,1,256]{2,1,0:T(1,128)S(1)} async-done(((f32[8,1,256]{2,1,0:T(1,128)}), f32[8,1,256]{2,1,0:T(1,128)S(1)}, u32[]{:S(2)}, u32[]{:S(2)}) %all-to-all-start) | async-done | bytes 8224 | tf_op jit(solution)/shard_map/all_to_all | solution.py:19
  64.6 0.4 convolution_convert_fusion
  65.0 0.8 copy.57
  65.8 3.7 %all-to-all-start.1 = ((bf16[8,128,256]{2,1,0:T(8,128)(2,1)}), bf16[8,128,256]{2,1,0:T(8,128)(2,1)S(1)}, u32[]{:S(2)}, u32[]{:S(2)}) async-start(bf16[8,128,256]{2,1,0:T(8,128)(2,1)} %bitcast.123), calls=%async_computation.1 | async-start | bytes 1048576 | tf_op jit(solution)/shard_map/all_to_all | solution.py:42
  69.5 1.2 reduce-window.6
  70.7 0.2 slice_reduce_fusion
  71.0 0.1 copy.42
  71.1 0.1 mul.809
  71.2 0.1 fusion.101
  71.3 2.4 scatter_custom_fusion
  73.8 7.1 %all-to-all-done.1 = bf16[8,128,256]{2,1,0:T(8,128)(2,1)S(1)} async-done(((bf16[8,128,256]{2,1,0:T(8,128)(2,1)}), bf16[8,128,256]{2,1,0:T(8,128)(2,1)S(1)}, u32[]{:S(2)}, u32[]{:S(2)}) %all-to-all-start.1) | async-done | bytes 524320 | tf_op jit(solution)/shard_map/all_to_all | solution.py:42
  80.9 0.1 convert_reduce_fusion
  80.9 0.1 fusion.36
  81.0 0.6 broadcast_in_dim.9
  81.7 4.3 %all-to-all-start.2 = ((f32[8,1,128]{2,1,0:T(1,128)}), f32[8,1,128]{2,1,0:T(1,128)S(1)}, u32[]{:S(2)}, u32[]{:S(2)}) async-start(f32[8,1,128]{2,1,0:T(1,128)} %broadcast_in_dim.9), calls=%async_computation.2 | async-start | bytes 8192 | tf_op jit(solution)/shard_map/all_to_all | solution.py:19
  86.0 0.8 dynamic_slice.3
  86.8 5.6 %all-to-all-done.2 = f32[8,1,128]{2,1,0:T(1,128)S(1)} async-done(((f32[8,1,128]{2,1,0:T(1,128)}), f32[8,1,128]{2,1,0:T(1,128)S(1)}, u32[]{:S(2)}, u32[]{:S(2)}) %all-to-all-start.2) | async-done | bytes 4128 | tf_op jit(solution)/shard_map/all_to_all | solution.py:19
  92.5 0.1 fusion.38
  92.6 3.9 %gather_fusion = bf16[1024,256]{1,0:T(8,128)(2,1)S(1)} fusion(bf16[129,256]{1,0:T(8,128)(2,1)S(1)} %concatenate.15, s32[1024]{0:T(1024)S(1)} %fusion.108), kind=kCustom, calls=%fused_computation | custom fusion | bytes 1052672 | tf_op jit(solution)/shard_map/gather | solution.py:121
  96.5 53.6 %all_to_all.27 = bf16[32,1,32,256]{3,2,1,0:T(8,128)(2,1)} all-to-all(bf16[32,1,32,256]{3,2,1,0:T(8,128)(2,1)S(1)} %bitcast.127), channel_id=1, replica_groups=mesh['grp'=2,'sp'=32,'tp'=8] {'sp'}, dimensions={0} | all-to-all | bytes 1048576 | tf_op jit(solution)/shard_map/all_to_all | solution.py:123
  150.2 54.3 %all-gather.3.cloned.1.call-done = bf16[32,1,32,2048]{3,2,0,1:T(8,128)(2,1)} async-done(((bf16[32,1,32,256]{3,2,0,1:T(8,128)(2,1)}), bf16[32,1,32,2048]{3,2,0,1:T(8,128)(2,1)}) %all-gather.3.cloned.1.call-update) | async-done | bytes 4194320 | tf_op jit(solution)/shard_map/all_gather | solution.py:122
  204.5 3.6 %fusion.9 = f32[32,1,32,256]{3,2,0,1:T(8,128)S(1)} fusion(bf16[32,1,32,2048]{3,2,0,1:T(8,128)(2,1)} %all-gather.3.cloned.1.call-done, bf16[1,2048,256]{2,1,0:T(8,128)(2,1)S(1)} %copy-done.7), kind=kOutput, calls=%fused_computation.11 | convolution fusion | flops 1074003968 | bytes 6291456 | tf_op jit(solution)/shard_map/slmd,ldf->slmf/dot_general | solution.py:128
  208.1 3.5 %fusion.24 = bf16[32,1,32,256]{3,2,0,1:T(8,128)(2,1)} fusion(bf16[32,1,32,2048]{3,2,0,1:T(8,128)(2,1)S(1)} %copy-done.6, bf16[1,2048,256]{2,1,0:T(8,128)(2,1)} %param.26, f32[32,1,32,256]{3,2,0,1:T(8,128)S(1)} %fusion.9), kind=kOutput, calls=%fused_computation.16 | convolution fusion | flops 1076101120 | bytes 6815744 | tf_op jit(solution)/shard_map/slmd,ldf->slmf/dot_general | solution.py:129
  211.7 67.7 %all-gather.5.cloned.1.call-done = bf16[32,1,32,2048]{3,2,0,1:T(8,128)(2,1)} async-done(((bf16[32,1,32,256]{3,2,0,1:T(8,128)(2,1)}), bf16[32,1,32,2048]{3,2,0,1:T(8,128)(2,1)}) %all-gather.5.cloned.1.call-update) | async-done | bytes 4194320 | tf_op jit(solution)/shard_map/all_gather | solution.py:133
  279.4 4.2 %fusion.30 = bf16[32,1,32,256]{3,2,1,0:T(8,128)(2,1)} fusion(bf16[32,1,32,2048]{3,2,0,1:T(8,128)(2,1)} %all-gather.5.cloned.1.call-done, bf16[1,2048,256]{2,1,0:T(8,128)(2,1)S(1)} %copy-done.8), kind=kOutput, calls=%fused_computation.18 | convolution fusion | flops 1074003968 | bytes 5767168 | tf_op jit(solution)/shard_map/slmf,lfd->slmd/dot_general | solution.py:131
  283.6 15.1 %all-to-all-start.4 = ((bf16[32,1,32,256]{3,2,1,0:T(8,128)(2,1)}), bf16[32,1,32,256]{3,2,1,0:T(8,128)(2,1)S(1)}, u32[]{:S(2)}, u32[]{:S(2)}) async-start(bf16[32,1,32,256]{3,2,1,0:T(8,128)(2,1)} %fusion.30), calls=%async_computation.4 | async-start | bytes 1048576 | tf_op jit(solution)/shard_map/all_to_all | solution.py:138
  298.7 0.1 copy.49
  298.8 33.2 %all-to-all-done.4 = bf16[32,1,32,256]{3,2,1,0:T(8,128)(2,1)S(1)} async-done(((bf16[32,1,32,256]{3,2,1,0:T(8,128)(2,1)}), bf16[32,1,32,256]{3,2,1,0:T(8,128)(2,1)S(1)}, u32[]{:S(2)}, u32[]{:S(2)}) %all-to-all-start.4) | async-done | bytes 524320 | tf_op jit(solution)/shard_map/all_to_all | solution.py:138
  332.0 1.9 gather_fusion.1
  334.0 0.1 reshape.145
  334.1 0.4 multiply_reduce_fusion
  334.5 0.6 fusion.39
  (39 shorter events, 0.5 us)
Async XLA Ops:
  6.5 58.0 %copy-start = (bf16[256,2048]{1,0:T(8,128)(2,1)S(1)}, bf16[256,2048]{1,0:T(8,128)(2,1)}, u32[]{:S(2)}) copy-start(bf16[256,2048]{1,0:T(8,128)(2,1)} %param.21) | copy-start | bytes 3145732
  6.6 51.6 %copy-start.2 = (s32[128,4]{0,1:T(4,128)S(1)}, s32[128,4]{0,1:T(4,128)}, u32[]{:S(2)}) copy-start(s32[128,4]{0,1:T(4,128)} %param.23) | copy-start | bytes 6148
  6.6 58.0 %copy-start.5 = (f32[256]{0:T(256)S(1)}, f32[256]{0:T(256)}, u32[]{:S(2)}) copy-start(f32[256]{0:T(256)} %param.18) | copy-start | bytes 3076
  6.6 58.0 %copy-start.4 = (f32[256]{0:T(256)S(1)}, f32[256]{0:T(256)}, u32[]{:S(2)}) copy-start(f32[256]{0:T(256)} %param.19) | copy-start | bytes 3076
  7.4 43.4 %collective-permute-start.1 = (s32[30]{0:T(128)S(1)}, s32[30]{0:T(128)S(1)}, u32[]{:S(2)}, u32[]{:S(2)}) collective-permute-start(s32[30]{0:T(128)S(1)} %slice.299), channel_id=1, source_target_pairs={{0,8},{8,16},{16,24},{24,32},{32,40},{40,48},{48,56},{56,64},{64,7... | collective-permute-start | bytes 368 | tf_op jit(solution)/shard_map/ppermute | solution.py:14
  15.4 37.6 %collective-permute-start = (bf16[30,256]{1,0:T(8,128)(2,1)S(1)}, bf16[30,256]{1,0:T(8,128)(2,1)S(1)}, u32[]{:S(2)}, u32[]{:S(2)}) collective-permute-start(bf16[30,256]{1,0:T(8,128)(2,1)S(1)} %slice.396), channel_id=1, source_target_pairs={{0,8},{8,16},{16,24},{24,32},{32,40},{40,48},{48,56},{56,64},{64,7... | collective-permute-start | bytes 46088 | tf_op jit(solution)/shard_map/ppermute | solution.py:14
  53.0 27.9 %copy-start.1 = (bf16[128,256]{1,0:T(8,128)(2,1)S(1)}, bf16[128,256]{1,0:T(8,128)(2,1)}, u32[]{:S(2)}) copy-start(bf16[128,256]{1,0:T(8,128)(2,1)} %param.20) | copy-start | bytes 196612
  54.6 9.9 %all-to-all-start = ((f32[8,1,256]{2,1,0:T(1,128)}), f32[8,1,256]{2,1,0:T(1,128)S(1)}, u32[]{:S(2)}, u32[]{:S(2)}) async-start(f32[8,1,256]{2,1,0:T(1,128)} %broadcast_in_dim.8), calls=%async_computation | async-start | bytes 16384 | tf_op jit(solution)/shard_map/all_to_all | solution.py:19
  65.8 15.1 %all-to-all-start.1 = ((bf16[8,128,256]{2,1,0:T(8,128)(2,1)}), bf16[8,128,256]{2,1,0:T(8,128)(2,1)S(1)}, u32[]{:S(2)}, u32[]{:S(2)}) async-start(bf16[8,128,256]{2,1,0:T(8,128)(2,1)} %bitcast.123), calls=%async_computation.1 | async-start | bytes 1048576 | tf_op jit(solution)/shard_map/all_to_all | solution.py:42
  69.5 135.0 %copy-start.7 = (bf16[1,2048,256]{2,1,0:T(8,128)(2,1)S(1)}, bf16[1,2048,256]{2,1,0:T(8,128)(2,1)}, u32[]{:S(2)}) copy-start(bf16[1,2048,256]{2,1,0:T(8,128)(2,1)} %param.25) | copy-start | bytes 3145732
  81.7 10.8 %all-to-all-start.2 = ((f32[8,1,128]{2,1,0:T(1,128)}), f32[8,1,128]{2,1,0:T(1,128)S(1)}, u32[]{:S(2)}, u32[]{:S(2)}) async-start(f32[8,1,128]{2,1,0:T(1,128)} %broadcast_in_dim.9), calls=%async_computation.2 | async-start | bytes 8192 | tf_op jit(solution)/shard_map/all_to_all | solution.py:19
  86.0 118.6 %all-gather.3.cloned.1.call-start = ((), (), s32[]{:S(2)}) async-start(), calls=%async_computation.5 | async-start | bytes 4718592 | tf_op jit(solution)/shard_map/all_gather | solution.py:122
  150.2 129.2 %all-gather.5.cloned.1.call-start = ((), (), s32[]{:S(2)}) async-start(), calls=%async_computation.6 | async-start | bytes 4718592 | tf_op jit(solution)/shard_map/all_gather | solution.py:133
  204.5 3.6 %copy-start.6 = (bf16[32,1,32,2048]{3,2,0,1:T(8,128)(2,1)S(1)}, bf16[32,1,32,2048]{3,2,0,1:T(8,128)(2,1)}, u32[]{:S(2)}) copy-start(bf16[32,1,32,2048]{3,2,0,1:T(8,128)(2,1)} %all-gather.3.cloned.1.call-done) | copy-start | bytes 12582916
  208.1 71.2 %copy-start.8 = (bf16[1,2048,256]{2,1,0:T(8,128)(2,1)S(1)}, bf16[1,2048,256]{2,1,0:T(8,128)(2,1)}, u32[]{:S(2)}) copy-start(bf16[1,2048,256]{2,1,0:T(8,128)(2,1)} %param.27) | copy-start | bytes 3145732
  211.7 87.0 %copy-start.3 = (f32[128,4]{0,1:T(4,128)S(1)}, f32[128,4]{0,1:T(4,128)}, u32[]{:S(2)}) copy-start(f32[128,4]{0,1:T(4,128)} %param.24) | copy-start | bytes 6148
  283.6 48.4 %all-to-all-start.4 = ((bf16[32,1,32,256]{3,2,1,0:T(8,128)(2,1)}), bf16[32,1,32,256]{3,2,1,0:T(8,128)(2,1)S(1)}, u32[]{:S(2)}, u32[]{:S(2)}) async-start(bf16[32,1,32,256]{3,2,1,0:T(8,128)(2,1)} %fusion.30), calls=%async_computation.4 | async-start | bytes 1048576 | tf_op jit(solution)/shard_map/all_to_all | solution.py:138
Sparse Core Ops, SparseCore 0:
  150.3 54.1 all-gather.2
  211.8 67.5 all-gather.4
where the time goes:
time: 343 us; the launch traced here: 342 us
  waiting for transfers between devices  205 us (60%)
  blocking collectives  53.6 us (16%)
  starting transfers between devices  35.7 us (10%)
  local copies, waits for them, and re-layouts  15 us (4%)
  between operations  13.7 us (4%)
  matrix products  11.7 us (3%)
  other arithmetic  6.8 us (2%)
    all_gather x1, waiting for transfers between devices, shards(): lax.all_gather(hidden, 'tp', axis=3, tiled=True)  67.7 us
    all_gather x1, waiting for transfers between devices, shards(): lax.all_gather(lax.all_to_all(packed, 'sp', split_axis=0, concat_axis=0,...  54.3 us
    all_to_all x1, blocking collectives, shards(): lax.all_to_all(packed, 'sp', split_axis=0, concat_axis=0, tiled=True)  53.6 us
    all_to_all x1, waiting for transfers between devices, shards(): lax.all_to_all(results, 'sp', split_axis=0, concat_axis=0, tiled=True)  33.2 us
    ppermute x2, waiting for transfers between devices, passed_along(): return lax.ppermute(array, axis, pairs)  31.5 us
    all_to_all x1, starting transfers between devices, shards(): lax.all_to_all(results, 'sp', split_axis=0, concat_axis=0, tiled=True)  15.1 us
    all_to_all x2, waiting for transfers between devices, copy_for_each(): return lax.all_to_all(copies, axis, split_axis=0, concat_axis=0, tiled=True)  11.7 us
    ppermute x2, starting transfers between devices, passed_along(): return lax.ppermute(array, axis, pairs)  9 us
  transfers between devices with their start and end apart: 8, of which 7 were waited for; matrix products, arithmetic and copies ran while one was open for 3% of the time, Pallas kernels for 0%

commit v1 on v0

--- a/solution.py
+++ b/solution.py
@@ -130,7 +130,15 @@
     hidden = clamped_unit(gate_pre, lin_pre).astype(jnp.bfloat16)
     summed = jnp.einsum(
         "slmf,lfd->slmd",
-        lax.all_gather(hidden, "tp", axis=3, tiled=True),
+        jnp.concatenate(
+            lax.all_to_all(
+                jnp.stack([hidden for _ in range(lax.axis_size("tp"))], axis=0),
+                axis_name="tp",
+                split_axis=0,
+                concat_axis=0,
+            ),
+            axis=3,
+        ),
         down_weight,
         preferred_element_type=jnp.float32,
     )

time: 343 us -> 383 us (1.12)
  blocking collectives: 53.6 us -> 146 us
  waiting for transfers between devices: 205 us -> 138 us
  local copies, waits for them, and re-layouts: 15 us -> 29.4 us
    all_to_all x0 -> x1, blocking collectives: none -> 92.8 us  [shards(): lax.all_to_all(jnp.stack([hidden for _ in range(lax.axis_size('tp'))], ax...]
    all_gather x1 -> x0, waiting for transfers between devices: 67.7 us -> none  [shards(): lax.all_gather(hidden, 'tp', axis=3, tiled=True)]
    another operation x1 -> x3, local copies, waits for them, and re-layouts: 0.01 us -> 8.03 us
    reshape x0 -> x1, local copies, waits for them, and re-layouts: none -> 6.25 us  [shards(): jnp.concatenate(lax.all_to_all(jnp.stack([hidden for _ in range(lax.axis_...]
  transfers between devices with their start and end apart: 8 -> 7, of which waited for: 7 -> 6; matrix products, arithmetic and copies ran while one was open for 3% -> 3% of each run, Pallas kernels for 0% -> 0%
where the time goes in v1:
time: 383 us; the launch traced here: 382 us
  blocking collectives  146 us (38%)
  waiting for transfers between devices  138 us (36%)
  starting transfers between devices  38.6 us (10%)
  local copies, waits for them, and re-layouts  29.4 us (8%)
  between operations  13.7 us (4%)
  matrix products  9.6 us (3%)
  other arithmetic  6.8 us (2%)
    all_to_all x1, blocking collectives, shards(): lax.all_to_all(jnp.stack([hidden for _ in range(lax.axis_size('tp'))], ax...  92.8 us
    all_gather x1, waiting for transfers between devices, shards(): lax.all_gather(lax.all_to_all(packed, 'sp', split_axis=0, concat_axis=0,...  54.4 us
    all_to_all x1, blocking collectives, shards(): lax.all_to_all(packed, 'sp', split_axis=0, concat_axis=0, tiled=True)  53.6 us
    all_to_all x1, waiting for transfers between devices, shards(): lax.all_to_all(results, 'sp', split_axis=0, concat_axis=0, tiled=True)  33.2 us
    ppermute x2, waiting for transfers between devices, passed_along(): return lax.ppermute(array, axis, pairs)  31.5 us
    all_to_all x1, starting transfers between devices, shards(): lax.all_to_all(results, 'sp', split_axis=0, concat_axis=0, tiled=True)  18 us
    all_to_all x2, waiting for transfers between devices, copy_for_each(): return lax.all_to_all(copies, axis, split_axis=0, concat_axis=0, tiled=True)  11.7 us
    ppermute x2, starting transfers between devices, passed_along(): return lax.ppermute(array, axis, pairs)  9 us
  transfers between devices with their start and end apart: 7, of which 6 were waited for; matrix products, arithmetic and copies ran while one was open for 3% of the time, Pallas kernels for 0%

profile of v1, /device:TPU:65, one launch (start us, length us, event | category | flops | bytes accessed | tf_op | source)
XLA Modules:
  0.0 382.2 jit_solution(6141006946376987191)
XLA Ops:
  6.6 0.8 slice.299
  7.4 7.0 %collective-permute-start.1 = (s32[30]{0:T(128)S(1)}, s32[30]{0:T(128)S(1)}, u32[]{:S(2)}, u32[]{:S(2)}) collective-permute-start(s32[30]{0:T(128)S(1)} %slice.299), channel_id=1, source_target_pairs={{0,8},{8,16},{16,24},{24,32},{32,40},{40,48},{48,56},{56,64},{64,7... | collective-permute-start | bytes 368 | tf_op jit(solution)/shard_map/ppermute | solution.py:14
  14.4 0.9 multiply_convert_fusion.1
  15.4 2.0 collective-permute-start
  17.3 1.0 fusion.113
  18.4 1.0 fusion.114
  19.3 31.4 %collective-permute-done.1 = s32[30]{0:T(128)S(1)} collective-permute-done((s32[30]{0:T(128)S(1)}, s32[30]{0:T(128)S(1)}, u32[]{:S(2)}, u32[]{:S(2)}) %collective-permute-start.1) | collective-permute-done | bytes 152 | tf_op jit(solution)/shard_map/ppermute | solution.py:14
  50.7 0.7 pad_add_fusion
  51.5 0.7 compare_convert_fusion.29
  52.2 0.7 compare_convert_fusion.28
  53.1 0.9 fusion.111
  54.0 0.6 broadcast_in_dim.8
  54.6 3.5 all-to-all-start
  58.2 0.1 copy.45
  58.4 0.1 eq.145
  58.5 6.0 %all-to-all-done = f32[8,1,256]{2,1,0:T(1,128)S(1)} async-done(((f32[8,1,256]{2,1,0:T(1,128)}), f32[8,1,256]{2,1,0:T(1,128)S(1)}, u32[]{:S(2)}, u32[]{:S(2)}) %all-to-all-start) | async-done | bytes 8224 | tf_op jit(solution)/shard_map/all_to_all | solution.py:19
  64.6 0.4 convolution_convert_fusion
  65.0 0.8 copy.60
  65.8 3.7 all-to-all-start.1
  69.5 1.2 reduce-window.6
  70.7 0.2 slice_reduce_fusion
  71.0 0.1 copy.44
  71.1 0.1 mul.809
  71.3 2.4 scatter_custom_fusion
  73.8 7.1 %all-to-all-done.1 = bf16[8,128,256]{2,1,0:T(8,128)(2,1)S(1)} async-done(((bf16[8,128,256]{2,1,0:T(8,128)(2,1)}), bf16[8,128,256]{2,1,0:T(8,128)(2,1)S(1)}, u32[]{:S(2)}, u32[]{:S(2)}) %all-to-all-start.1) | async-done | bytes 524320 | tf_op jit(solution)/shard_map/all_to_all | solution.py:42
  80.9 0.1 fusion.32
  81.1 0.6 broadcast_in_dim.9
  81.7 4.3 %all-to-all-start.2 = ((f32[8,1,128]{2,1,0:T(1,128)}), f32[8,1,128]{2,1,0:T(1,128)S(1)}, u32[]{:S(2)}, u32[]{:S(2)}) async-start(f32[8,1,128]{2,1,0:T(1,128)} %broadcast_in_dim.9), calls=%async_computation.2 | async-start | bytes 8192 | tf_op jit(solution)/shard_map/all_to_all | solution.py:19
  86.0 0.8 dynamic_slice.3
  86.8 5.6 %all-to-all-done.2 = f32[8,1,128]{2,1,0:T(1,128)S(1)} async-done(((f32[8,1,128]{2,1,0:T(1,128)}), f32[8,1,128]{2,1,0:T(1,128)S(1)}, u32[]{:S(2)}, u32[]{:S(2)}) %all-to-all-start.2) | async-done | bytes 4128 | tf_op jit(solution)/shard_map/all_to_all | solution.py:19
  92.6 3.9 %gather_fusion = bf16[1024,256]{1,0:T(8,128)(2,1)S(1)} fusion(bf16[129,256]{1,0:T(8,128)(2,1)S(1)} %concatenate.15, s32[1024]{0:T(1024)S(1)} %fusion.104), kind=kCustom, calls=%fused_computation | custom fusion | bytes 1052672 | tf_op jit(solution)/shard_map/gather | solution.py:121
  96.5 53.6 %all_to_all.32 = bf16[32,1,32,256]{3,2,1,0:T(8,128)(2,1)} all-to-all(bf16[32,1,32,256]{3,2,1,0:T(8,128)(2,1)S(1)} %bitcast.133), channel_id=1, replica_groups=mesh['grp'=2,'sp'=32,'tp'=8] {'sp'}, dimensions={0} | all-to-all | bytes 1048576 | tf_op jit(solution)/shard_map/all_to_all | solution.py:123
  150.2 54.4 %all-gather.2.cloned.1.call-done = bf16[32,1,32,2048]{3,2,0,1:T(8,128)(2,1)} async-done(((bf16[32,1,32,256]{3,2,0,1:T(8,128)(2,1)}), bf16[32,1,32,2048]{3,2,0,1:T(8,128)(2,1)}) %all-gather.2.cloned.1.call-update) | async-done | bytes 4194320 | tf_op jit(solution)/shard_map/all_gather | solution.py:122
  204.5 3.6 fusion.7
  208.2 0.1 copy-done.8
  208.3 1.4 fusion.26
  209.7 0.5 stack.2
  210.2 92.8 %all_to_all.33 = bf16[8,32,1,32,256]{4,3,1,2,0:T(8,128)(2,1)S(1)} all-to-all(bf16[8,32,1,32,256]{4,3,1,2,0:T(8,128)(2,1)S(1)} %stack.2), channel_id=1, replica_groups=mesh['grp'=2,'sp'=32,'tp'=8] {'tp'}, dimensions={0} | all-to-all | bytes 8388608 | tf_op jit(solution)/shard_map/all_to_all | solution.py:134
  303.0 6.3 %copy.50 = bf16[32,1,32,8,256]{4,3,2,0,1:T(8,128)(2,1)} copy(bf16[32,1,32,8,256]{4,2,0,1,3:T(8,128)(2,1)S(1)} %bitcast.129) | data formatting | bytes 8388608 | tf_op jit(solution)/shard_map/reshape | solution.py:133
  309.2 7.5 %reshape.151 = bf16[32,32,2048]{2,1,0:T(8,128)(2,1)} reshape(bf16[32,1,32,8,256]{4,3,2,0,1:T(8,128)(2,1)} %copy.50) | data formatting | bytes 8388608 | tf_op jit(solution)/shard_map/reshape.18
  316.7 4.2 %fusion.25 = bf16[32,1,32,256]{3,2,1,0:T(8,128)(2,1)} fusion(bf16[32,32,2048]{2,1,0:T(8,128)(2,1)} %reshape.151, bf16[1,2048,256]{2,1,0:T(8,128)(2,1)S(1)} %copy-done.9), kind=kOutput, calls=%fused_computation.16 | convolution fusion | flops 1074003968 | bytes 5767168 | tf_op jit(solution)/shard_map/slmf,lfd->slmd/dot_general | solution.py:131
  321.0 18.0 %all-to-all-start.5 = ((bf16[32,1,32,256]{3,2,1,0:T(8,128)(2,1)}), bf16[32,1,32,256]{3,2,1,0:T(8,128)(2,1)S(1)}, u32[]{:S(2)}, u32[]{:S(2)}) async-start(bf16[32,1,32,256]{3,2,1,0:T(8,128)(2,1)} %fusion.25), calls=%async_computation.5 | async-start | bytes 1048576 | tf_op jit(solution)/shard_map/all_to_all | solution.py:146
  339.0 0.1 copy.52
  339.1 33.2 %all-to-all-done.5 = bf16[32,1,32,256]{3,2,1,0:T(8,128)(2,1)S(1)} async-done(((bf16[32,1,32,256]{3,2,1,0:T(8,128)(2,1)}), bf16[32,1,32,256]{3,2,1,0:T(8,128)(2,1)S(1)}, u32[]{:S(2)}, u32[]{:S(2)}) %all-to-all-start.5) | async-done | bytes 524320 | tf_op jit(solution)/shard_map/all_to_all | solution.py:146
  372.3 1.9 gather_fusion.1
  374.2 0.1 reshape.154
  374.3 0.4 multiply_reduce_fusion
  374.7 0.6 fusion.35
  (42 shorter events, 0.7 us)
Async XLA Ops:
  6.5 58.0 %copy-start = (bf16[256,2048]{1,0:T(8,128)(2,1)S(1)}, bf16[256,2048]{1,0:T(8,128)(2,1)}, u32[]{:S(2)}) copy-start(bf16[256,2048]{1,0:T(8,128)(2,1)} %param.21) | copy-start | bytes 3145732
  6.6 51.6 %copy-start.2 = (s32[128,4]{0,1:T(4,128)S(1)}, s32[128,4]{0,1:T(4,128)}, u32[]{:S(2)}) copy-start(s32[128,4]{0,1:T(4,128)} %param.23) | copy-start | bytes 6148
  6.6 58.0 %copy-start.5 = (f32[256]{0:T(256)S(1)}, f32[256]{0:T(256)}, u32[]{:S(2)}) copy-start(f32[256]{0:T(256)} %param.18) | copy-start | bytes 3076
  6.6 58.0 %copy-start.4 = (f32[256]{0:T(256)S(1)}, f32[256]{0:T(256)}, u32[]{:S(2)}) copy-start(f32[256]{0:T(256)} %param.19) | copy-start | bytes 3076
  7.4 43.4 %collective-permute-start.1 = (s32[30]{0:T(128)S(1)}, s32[30]{0:T(128)S(1)}, u32[]{:S(2)}, u32[]{:S(2)}) collective-permute-start(s32[30]{0:T(128)S(1)} %slice.299), channel_id=1, source_target_pairs={{0,8},{8,16},{16,24},{24,32},{32,40},{40,48},{48,56},{56,64},{64,7... | collective-permute-start | bytes 368 | tf_op jit(solution)/shard_map/ppermute | solution.py:14
  15.4 37.6 %collective-permute-start = (bf16[30,256]{1,0:T(8,128)(2,1)S(1)}, bf16[30,256]{1,0:T(8,128)(2,1)S(1)}, u32[]{:S(2)}, u32[]{:S(2)}) collective-permute-start(bf16[30,256]{1,0:T(8,128)(2,1)S(1)} %slice.396), channel_id=1, source_target_pairs={{0,8},{8,16},{16,24},{24,32},{32,40},{40,48},{48,56},{56,64},{64,7... | collective-permute-start | bytes 46088 | tf_op jit(solution)/shard_map/ppermute | solution.py:14
  53.0 27.9 %copy-start.1 = (bf16[128,256]{1,0:T(8,128)(2,1)S(1)}, bf16[128,256]{1,0:T(8,128)(2,1)}, u32[]{:S(2)}) copy-start(bf16[128,256]{1,0:T(8,128)(2,1)} %param.20) | copy-start | bytes 196612
  54.6 9.9 %all-to-all-start = ((f32[8,1,256]{2,1,0:T(1,128)}), f32[8,1,256]{2,1,0:T(1,128)S(1)}, u32[]{:S(2)}, u32[]{:S(2)}) async-start(f32[8,1,256]{2,1,0:T(1,128)} %broadcast_in_dim.8), calls=%async_computation | async-start | bytes 16384 | tf_op jit(solution)/shard_map/all_to_all | solution.py:19
  65.8 15.1 %all-to-all-start.1 = ((bf16[8,128,256]{2,1,0:T(8,128)(2,1)}), bf16[8,128,256]{2,1,0:T(8,128)(2,1)S(1)}, u32[]{:S(2)}, u32[]{:S(2)}) async-start(bf16[8,128,256]{2,1,0:T(8,128)(2,1)} %bitcast.128), calls=%async_computation.1 | async-start | bytes 1048576 | tf_op jit(solution)/shard_map/all_to_all | solution.py:42
  69.5 135.0 %copy-start.7 = (bf16[1,2048,256]{2,1,0:T(8,128)(2,1)S(1)}, bf16[1,2048,256]{2,1,0:T(8,128)(2,1)}, u32[]{:S(2)}) copy-start(bf16[1,2048,256]{2,1,0:T(8,128)(2,1)} %param.25) | copy-start | bytes 3145732
  81.7 10.8 %all-to-all-start.2 = ((f32[8,1,128]{2,1,0:T(1,128)}), f32[8,1,128]{2,1,0:T(1,128)S(1)}, u32[]{:S(2)}, u32[]{:S(2)}) async-start(f32[8,1,128]{2,1,0:T(1,128)} %broadcast_in_dim.9), calls=%async_computation.2 | async-start | bytes 8192 | tf_op jit(solution)/shard_map/all_to_all | solution.py:19
  86.0 118.6 %all-gather.2.cloned.1.call-start = ((), (), s32[]{:S(2)}) async-start(), calls=%async_computation.6 | async-start | bytes 4718592 | tf_op jit(solution)/shard_map/all_gather | solution.py:122
  204.5 3.6 copy-start.6
  204.5 3.7 copy-start.8
  309.2 7.5 %copy-start.9 = (bf16[1,2048,256]{2,1,0:T(8,128)(2,1)S(1)}, bf16[1,2048,256]{2,1,0:T(8,128)(2,1)}, u32[]{:S(2)}) copy-start(bf16[1,2048,256]{2,1,0:T(8,128)(2,1)} %param.27) | copy-start | bytes 3145732
  316.7 22.2 %copy-start.3 = (f32[128,4]{0,1:T(4,128)S(1)}, f32[128,4]{0,1:T(4,128)}, u32[]{:S(2)}) copy-start(f32[128,4]{0,1:T(4,128)} %param.24) | copy-start | bytes 6148
  321.0 51.3 %all-to-all-start.5 = ((bf16[32,1,32,256]{3,2,1,0:T(8,128)(2,1)}), bf16[32,1,32,256]{3,2,1,0:T(8,128)(2,1)S(1)}, u32[]{:S(2)}, u32[]{:S(2)}) async-start(bf16[32,1,32,256]{3,2,1,0:T(8,128)(2,1)} %fusion.25), calls=%async_computation.5 | async-start | bytes 1048576 | tf_op jit(solution)/shard_map/all_to_all | solution.py:146
Sparse Core Ops, SparseCore 0:
  150.3 54.2 all-gather.1
